TPU v7x, 256 devices: a whole 4x4x8 slice. The times are simulated.
256 devices in a mesh: ep: 64 (over z, y, core), tp: 4 (over x).
Axes of the slice: x: 4, y: 4, z: 8, core: 2. Of those that a mesh axis runs over, the one named last changes fastest.
Arguments:
- state_probe_logits: bfloat16 [65536, 1024], P('ep', 'tp'), may hold values from -6 to 6
- retention_logits: bfloat16 [65536, 1024], P('ep', 'tp'), may hold values from -12 to 12
- state_source_entries: bfloat16 [65536, 1024], P('ep', 'tp'), may hold values from -6 to 6
- state_result_switch_logits: bfloat16 [65536, 1024], P('ep', 'tp'), may hold values from -6 to 6
- retention_bound_margin: float32 [1024], P('tp'), may hold values from 0 to 0.07
- extra_fading_amount: float32 [65536, 8], P('ep', 'tp'), may hold values from -0.7 to 0
- state_result_scale: float32 [1024], P('tp'), may hold values from 0.1 to 1.9
- state_result_matrix: bfloat16 [1024, 2048], P(None, 'tp'), may hold values from -0.1875 to 0.1875
- second_slice_tokens: bfloat16 [32768, 2048], P('ep'), may hold values from -6 to 6
- specialist_assignment: int32 [32768, 2], P('ep'), may hold values from 0 to 63, all different within a row; in each aligned block of 128 rows (0 to 127, 128 to 255, ...) at most 8 rows name the same one
- selected_specialist_share: float32 [32768, 2], P('ep'), may hold values from 0.1 to 1
- leading_scale_vector: float32 [2048], replicated, may hold values from 0.1 to 1.9
- trailing_scale_vector: float32 [2048], replicated, may hold values from 0.1 to 1.9
- specialist_switch_matrix: bfloat16 [64, 2048, 2048], P('ep', None, 'tp'), may hold values from -0.3125 to 0.3125
- specialist_widen_matrix: bfloat16 [64, 2048, 2048], P('ep', None, 'tp'), may hold values from -0.3125 to 0.3125
- specialist_contract_matrix: bfloat16 [64, 2048, 2048], P('ep', 'tp'), may hold values from -0.125 to 0.125
Outputs:
- mixer_out: bfloat16 [65536, 2048], P('ep', 'tp')
- moe_out: bfloat16 [32768, 2048], P(('ep', 'tp'))
Inputs may be any that keep to these rules, and one draw needn't show every extreme that they name: `specialist_assignment`: each row names 2 different experts. In each aligned block of 128 rows no expert is named by more than 8 rows, a bound that some block reaches.
All inputs are finite; a program needn't handle non-finite values.
Results may differ from a plain program's by a relative error of at most 0.012.
Values may be sent and summed in bfloat16 or wider, within the bound.
No kernel may reach another device: no remote copies, remote signals or barrier semaphores. Data moves between devices by JAX's collectives and lax.ppermute only.
A program may use at most 128 MiB of HBM per device.

v0:
```python
import jax
import jax.numpy as jnp
from jax import lax
from jax.sharding import Mesh
from jax.sharding import PartitionSpec as P

HEAD = 128
SPAN_STEPS = 64
TOK_DEV = 128
EP = ("ep_0", "ep_1", "ep_2")
EP_TP = ("ep_0", "ep_1", "ep_2", "tp")
NORM_EPS = 1e-06
SWISH_ALPHA = 1.702
CLAMP_LIMIT = 7.0


def sent_to_all(shard, axis):
    length = lax.axis_size(axis)
    return lax.all_to_all(
        jnp.broadcast_to(shard[None], (length, *shard.shape)), axis, 0, 0, tiled=True
    )


def joined_along(tiles, dim):
    shape = list(tiles.shape[1:])
    shape[dim] *= tiles.shape[0]
    return jnp.moveaxis(tiles, 0, dim).reshape(shape)


def gathered_copies(shard, axis, dim):
    tiles = sent_to_all(shard, axis)
    return joined_along(tiles, dim)


def all_blocks(shard, axes, order):
    tiles = shard[None]
    for k in order:
        tiles = lax.all_gather(tiles, axes[k], axis=0, tiled=True)
    current = [lax.axis_size(axes[k]) for k in reversed(order)]
    tiles = tiles.reshape(*current, *shard.shape)
    turned = sorted(range(len(order)), key=lambda place: order[len(order) - 1 - place])
    return tiles.transpose(*turned, *range(len(order), tiles.ndim)).reshape(-1, *shard.shape)


def gather_axes(shard, axes, order, dim):
    return joined_along(all_blocks(shard, axes, order), dim)


def in_blocks(shard, dim, length):
    before, after = (shard.shape[:dim], shard.shape[dim + 1 :])
    return jnp.moveaxis(shard.reshape(*before, length, -1, *after), dim, 0)


def sum_at_owner(shard, axis, dim):
    length = lax.axis_size(axis)
    tiles = lax.all_to_all(in_blocks(shard, dim, length), axis, 0, 0, tiled=True)
    return jnp.sum(tiles.astype(jnp.float32), axis=0)


def rms_scale(values, gain):
    return values * lax.rsqrt(jnp.mean(values * values, axis=-1, keepdims=True) + NORM_EPS) * gain


def clamped_unit(gate, upward):
    glued = jnp.minimum(gate, CLAMP_LIMIT)
    linear = jnp.clip(upward, -CLAMP_LIMIT, CLAMP_LIMIT)
    return glued * jax.nn.sigmoid(SWISH_ALPHA * glued) * (linear + 1.0)


def slot_table(routes, quarters, experts, capacity):
    per_quarter = routes.shape[0] * routes.shape[1] // quarters
    flat = routes.reshape(quarters, per_quarter)
    onehot = (flat[:, :, None] == jnp.arange(experts, dtype=jnp.int32)[None, None, :]).astype(
        jnp.int32
    )
    rank = jnp.sum(onehot * (jnp.cumsum(onehot, axis=1) - 1), axis=2)
    quarter_ids = jnp.arange(quarters, dtype=jnp.int32)[:, None]
    return ((quarter_ids * experts + flat) * capacity + rank).reshape(-1)


def pack_rows(normed, routes, quarters, experts, capacity):
    slots = slot_table(routes, quarters, experts, capacity)
    room = quarters * experts * capacity
    owner = jnp.arange(slots.shape[0], dtype=jnp.int32) // routes.shape[1]
    source = jnp.zeros((room,), jnp.int32).at[slots].set(owner)
    filled = jnp.zeros((room,), jnp.bool_).at[slots].set(True)
    packed = jnp.where(filled[:, None], normed[source], jnp.zeros((), jnp.bfloat16))
    return packed.reshape(quarters, experts, capacity, normed.shape[1])


def shards(
    state_probe_logits,
    retention_logits,
    state_source_entries,
    state_result_switch_logits,
    retention_bound_margin,
    extra_fading_amount,
    state_result_scale,
    state_result_matrix,
    second_slice_tokens,
    specialist_assignment,
    selected_specialist_share,
    leading_scale_vector,
    trailing_scale_vector,
    specialist_switch_matrix,
    specialist_widen_matrix,
    specialist_contract_matrix,
):
    total_rows, width = state_probe_logits.shape
    groups_each_device = width // HEAD
    span_tally = total_rows // SPAN_STEPS

    def per_head(values):
        return values.reshape(span_tally, SPAN_STEPS, groups_each_device, HEAD).transpose(
            0, 2, 1, 3
        )

    query = per_head(jax.nn.silu(state_probe_logits.astype(jnp.float32)) * HEAD ** (-0.5))
    input_key = per_head(
        retention_bound_margin * jax.nn.sigmoid(-retention_logits.astype(jnp.float32))
    )
    decay_logarithm = (
        jnp.log1p(-input_key)
        + extra_fading_amount.reshape(span_tally, SPAN_STEPS, groups_each_device).transpose(
            0, 2, 1
        )[..., None]
    )
    values = per_head(state_source_entries.astype(jnp.float32))
    cumul = jnp.cumsum(decay_logarithm, axis=2)
    middle = cumul[:, :, SPAN_STEPS // 2 - 1 : SPAN_STEPS // 2]
    last = cumul[:, :, SPAN_STEPS - 1 :]
    causal = jnp.tril(jnp.ones((SPAN_STEPS, SPAN_STEPS), jnp.float32))
    scores = (
        jnp.einsum(
            "nhid,nhjd->nhij", query * jnp.exp(cumul - middle), input_key * jnp.exp(middle - cumul)
        )
        * causal
    )
    inner = jnp.einsum("nhij,nhje->nhie", scores, values)
    update = jnp.einsum("nhcd,nhce->nhde", input_key * jnp.exp(last - cumul), values)
    block_decay = last[:, :, 0]

    def advance(state, operand_tensors):
        decay_log, addition = operand_tensors
        return (jnp.exp(decay_log)[..., None] * state + addition, state)

    end_state, local_start = lax.scan(
        advance, jnp.zeros((groups_each_device, HEAD, HEAD), jnp.float32), (block_decay, update)
    )
    decay_total = jnp.sum(block_decay, axis=0)
    running = jnp.cumsum(block_decay, axis=0)
    before = jnp.concatenate([jnp.zeros_like(running[:1]), running[:-1]], axis=0)
    totals = gathered_copies(decay_total[None], EP, 0)
    through = jnp.cumsum(totals, axis=0)
    my_index = lax.axis_index(EP)
    reach = lax.dynamic_index_in_dim(through - totals, my_index, 0, keepdims=False)
    portion = gather_axes(end_state[None].astype(jnp.bfloat16), EP, (1, 0, 2), 0).astype(
        jnp.float32
    )
    length = portion.shape[0]
    earlier = jnp.arange(length, dtype=jnp.int32) < my_index
    weights = jnp.where(
        earlier[:, None, None], jnp.exp(jnp.minimum(reach[None] - through, 0.0)), 0.0
    )
    entering = jnp.zeros_like(end_state) + jnp.einsum("jhd,jhde->hde", weights, portion)
    start_state = local_start + jnp.exp(before)[..., None] * entering[None]
    outer = jnp.einsum("nhcd,nhde->nhce", query * jnp.exp(cumul), start_state)
    raw_out = inner + outer
    normed_rec = raw_out * lax.rsqrt(jnp.mean(raw_out * raw_out, axis=-1, keepdims=True) + NORM_EPS)
    normed_rec = normed_rec.transpose(0, 2, 1, 3).reshape(total_rows, width)
    state_layer_result = (
        normed_rec
        * state_result_scale
        * jax.nn.silu(state_result_switch_logits.astype(jnp.float32))
    ).astype(jnp.bfloat16)
    mixed = jnp.dot(
        lax.all_gather(state_layer_result, "tp", axis=1, tiled=True),
        state_result_matrix,
        preferred_element_type=jnp.float32,
    )
    mixer_out = mixed.astype(jnp.bfloat16)
    experts = specialist_switch_matrix.shape[0] * lax.axis_size(EP)
    top_count = specialist_assignment.shape[1]
    capacity = 2 * TOK_DEV * top_count // experts
    my_quarter = lax.axis_index("tp")
    own_route = lax.dynamic_slice_in_dim(specialist_assignment, my_quarter * TOK_DEV, TOK_DEV, 0)
    own_weight = lax.dynamic_slice_in_dim(
        selected_specialist_share, my_quarter * TOK_DEV, TOK_DEV, 0
    )
    own_rows = lax.dynamic_slice_in_dim(second_slice_tokens, my_quarter * TOK_DEV, TOK_DEV, 0)
    normed = rms_scale(own_rows.astype(jnp.float32), leading_scale_vector).astype(jnp.bfloat16)
    packed = pack_rows(normed, own_route, 1, experts, capacity)[0]
    arrived = lax.all_to_all(packed, EP, split_axis=0, concat_axis=0, tiled=True)
    portion = lax.all_gather(arrived.reshape(-1, arrived.shape[2]), "tp", axis=0, tiled=True)
    gate = jnp.dot(portion, specialist_switch_matrix[0], preferred_element_type=jnp.float32)
    upward = jnp.dot(portion, specialist_widen_matrix[0], preferred_element_type=jnp.float32)
    activated = clamped_unit(gate, upward).astype(jnp.bfloat16)
    summed = sum_at_owner(
        jnp.dot(
            activated, specialist_contract_matrix[0], preferred_element_type=jnp.float32
        ).astype(jnp.bfloat16),
        "tp",
        0,
    )
    finished = summed.astype(jnp.bfloat16).reshape(-1, capacity, summed.shape[1])
    returned = lax.all_to_all(finished, EP, split_axis=0, concat_axis=0, tiled=True)
    flat_back = returned.reshape(-1, returned.shape[2])
    own_slots = slot_table(own_route, 1, experts, capacity).reshape(TOK_DEV, top_count)
    combined = jnp.zeros((TOK_DEV, flat_back.shape[1]), jnp.float32)
    for column in range(top_count):
        combined = (
            combined
            + flat_back[own_slots[:, column]].astype(jnp.float32)
            * own_weight[:, column : column + 1]
        )
    moe_out = rms_scale(combined, trailing_scale_vector).astype(jnp.bfloat16)
    return (mixer_out, moe_out)


def solution(mesh):
    finer = Mesh(mesh.devices.reshape(8, 4, 2, mesh.shape["tp"]), ("ep_0", "ep_1", "ep_2", "tp"))
    placed = (
        P(EP, "tp"),
        P(EP, "tp"),
        P(EP, "tp"),
        P(EP, "tp"),
        P("tp"),
        P(EP, "tp"),
        P("tp"),
        P(None, "tp"),
        P(EP, None),
        P(EP, None),
        P(EP, None),
        P(),
        P(),
        P(EP, None, "tp"),
        P(EP, None, "tp"),
        P(EP, "tp", None),
    )
    return jax.shard_map(
        shards,
        mesh=finer,
        in_specs=placed,
        out_specs=(P(EP, "tp"), P(EP_TP, None)),
        check_vma=False,
    )
```

profile of v0, /device:TPU:8, one launch (start us, length us, event | category | flops | bytes accessed | tf_op | source)
XLA Modules:
  0.0 367.5 jit_solution(13056595619154716890)
XLA Ops:
  10.0 1.4 scatter_custom_fusion.1
  12.7 1.5 scatter_custom_fusion
  14.3 1.3 fusion.19
  15.5 3.3 gather_fusion
  18.9 1.8 bitcast_select_fusion
  20.7 63.2 %all_to_all.20 = bf16[64,8,2048]{2,1,0:T(8,128)(2,1)} all-to-all(bf16[64,8,2048]{2,1,0:T(8,128)(2,1)S(1)} %bitcast_select_fusion), channel_id=1, replica_groups=mesh['ep_0'=8,'ep_1'=4,'ep_2'=2,'tp'=4] {'ep_0','ep_1','ep_2'}, dimensions={0} | all-to-all | bytes 4194304 | tf_op jit(solution)/shard_map/all_to_all | solution.py:193
  86.2 1.7 reshape.256
  90.6 5.4 %all-to-all-start = ((f32[64,1,2,128]{3,2,1,0:T(2,128)}), f32[64,1,2,128]{3,2,1,0:T(2,128)S(1)}, u32[]{:S(2)}, u32[]{:S(2)}) async-start(f32[64,1,2,128]{3,2,1,0:T(2,128)} %broadcast_in_dim.86), calls=%async_computation | async-start | bytes 131072 | tf_op jit(solution)/shard_map/all_to_all | solution.py:19
  96.1 2.3 fusion.12
  98.5 2.7 reshape.255
  101.2 2.0 reshape.258
  103.2 4.3 %bitcast_multiply_fusion.5 = (bf16[16,2,64,128]{3,0,1,2:T(8,128)(2,1)}, bf16[16,2,64,128]{3,0,1,2:T(8,128)(2,1)}, bf16[16,2,64,128]{3,0,1,2:T(8,128)(2,1)S(1)}, bf16[16,2,64,128]{3,0,1,2:T(8,128)(2,1)}) fusion(f32[16,2,64,128]{3,0,1,2:T(8,128)} %copy-done.5, f32[16,64,2,128]{3,2,1,0:T(2,128)} %reshape.255, f32[16,2,128]{2,0,1:T(8,128)S(1)} %get-tuple-element.88, ...), kind=kLoop, calls=%fused_computation.49 | loop fusion | flops 2883584 | bytes 5275648 | tf_op jit(solution)/shard_map/mul | solution.py:135
  107.5 1.8 fusion.25
  109.3 27.5 %while.13 = (s32[]{:T(128)}, f32[2,128,128]{2,1,0:T(8,128)S(1)}, f32[16,2,128,128]{3,2,1,0:T(8,128)}, f32[16,2,128]{2,1,0:T(2,128)S(1)}, f32[16,2,128,128]{3,2,1,0:T(8,128)}, /*index=5*/s32[]{:T(128)}, s32[]{:T(128)}) while((s32[]{:T(128)}, f32[2,128,128]{2,1,0:T(8,128)S(1)}, f32[16,2,128,128]{3,2,1,0:T(8,128)}, ...), condition=%wide.region_2.3_spmd.clone, body=%wide.region_1.2_spmd.clone.sunk | while | flops 131075 | bytes 659040 | solution.py:147
  136.8 13.2 %all-gather = bf16[8,128,128]{2,1,0:T(8,128)(2,1)} all-gather(bf16[2,128,128]{2,1,0:T(8,128)(2,1)S(1)} %convert_element_type.56), channel_id=2, replica_groups=mesh['ep_0'=8,'ep_1'=4,'ep_2'=2,'tp'=4] {'ep_1'}, dimensions={0}, use_global_device_ids=true | all-gather | bytes 327680 | tf_op jit(solution)/shard_map/all_gather | solution.py:38
  150.0 15.9 %all-gather.12.cloned.1.call-done = bf16[2048,2048]{1,0:T(8,128)(2,1)} async-done(((bf16[512,2048]{1,0:T(8,128)(2,1)}), bf16[2048,2048]{1,0:T(8,128)(2,1)}) %all-gather.12.cloned.1.call-update) | async-done | bytes 8388624 | tf_op jit(solution)/shard_map/all_gather | solution.py:194
  165.9 7.7 %fusion.4 = f32[2048,512]{1,0:T(8,128)S(1)} fusion(bf16[2048,2048]{1,0:T(8,128)(2,1)} %all-gather.12.cloned.1.call-done, bf16[1,2048,512]{2,1,0:T(8,128)(2,1)} %param.31), kind=kOutput, calls=%fused_computation.14 | convolution fusion | flops 4294967296 | bytes 14680064 | tf_op jit(solution)/shard_map/dot_general | solution.py:195
  173.6 5.6 %multiply_convert_fusion = bf16[2048,512]{1,0:T(8,128)(2,1)S(1)} fusion(f32[2048,512]{1,0:T(8,128)S(1)} %fusion.4, bf16[2048,2048]{1,0:T(8,128)(2,1)S(1)} %copy-done.15, bf16[1,2048,512]{2,1,0:T(8,128)(2,1)S(1)} %copy-done.16), kind=kOutput, calls=%fused_computation.11 | convolution fusion | flops 4305453056 | bytes 16777216 | tf_op jit(solution)/shard_map/dot_general | solution.py:196
  179.2 6.7 %convolution_convert_fusion = bf16[2048,2048]{1,0:T(8,128)(2,1)} fusion(bf16[2048,512]{1,0:T(8,128)(2,1)S(1)} %multiply_convert_fusion, bf16[1,512,2048]{2,1,0:T(8,128)(2,1)S(1)} %copy-done), kind=kOutput, calls=%fused_computation.8 | convolution fusion | flops 4299161600 | bytes 12582912 | tf_op jit(solution)/shard_map/dot_general | solution.py:199
  186.0 5.7 %all-to-all-start.2 = ((bf16[4,512,2048]{2,1,0:T(8,128)(2,1)}), bf16[4,512,2048]{2,1,0:T(8,128)(2,1)}, u32[]{:S(2)}, u32[]{:S(2)}) async-start(bf16[4,512,2048]{2,1,0:T(8,128)(2,1)} %bitcast.107), calls=%async_computation.2 | async-start | bytes 16777216 | tf_op jit(solution)/shard_map/all_to_all | solution.py:56
  191.7 17.9 %all-gather.6.cloned.1.call-done = bf16[32,1,2,128,128]{4,3,2,1,0:T(8,128)(2,1)} async-done(((bf16[4,1,2,128,128]{4,3,2,1,0:T(8,128)(2,1)}), bf16[32,1,2,128,128]{4,3,2,1,0:T(8,128)(2,1)}) %all-gather.6.cloned.1.call-update) | async-done | bytes 2097168 | tf_op jit(solution)/shard_map/all_gather | solution.py:38
  210.0 18.9 %all-gather.8.cloned.1.call-done = bf16[64,1,2,128,128]{4,3,2,1,0:T(8,128)(2,1)} async-done(((bf16[32,1,2,128,128]{4,3,2,1,0:T(8,128)(2,1)}), bf16[64,1,2,128,128]{4,3,2,1,0:T(8,128)(2,1)}) %all-gather.8.cloned.1.call-update) | async-done | bytes 4194320 | tf_op jit(solution)/shard_map/all_gather | solution.py:38
  229.0 2.5 copy.63
  231.5 2.8 fusion
  235.5 1.9 multiply_reduce_fusion.1
  237.4 48.2 %all-to-all-done.2 = bf16[4,512,2048]{2,1,0:T(8,128)(2,1)} async-done(((bf16[4,512,2048]{2,1,0:T(8,128)(2,1)}), bf16[4,512,2048]{2,1,0:T(8,128)(2,1)}, u32[]{:S(2)}, u32[]{:S(2)}) %all-to-all-start.2) | async-done | bytes 8388640 | tf_op jit(solution)/shard_map/all_to_all | solution.py:56
  285.6 7.3 %reduce_sum.70 = bf16[512,2048]{1,0:T(8,128)(2,1)} reduce(bf16[4,512,2048]{2,1,0:T(8,128)(2,1)} %all-to-all-done.2, bf16[]{:T(256)} %constant.117.clone.1), dimensions={0}, to_apply=%region_13.14 | reduce | flops 3145728 | bytes 10485762 | tf_op jit(solution)/shard_map/reduce_sum | solution.py:57
  292.8 10.6 %all-to-all-start.3 = ((bf16[64,8,2048]{2,1,0:T(8,128)(2,1)}), bf16[64,8,2048]{2,1,0:T(8,128)(2,1)S(1)}, u32[]{:S(2)}, u32[]{:S(2)}) async-start(bf16[64,8,2048]{2,1,0:T(8,128)(2,1)} %bitcast.109), calls=%async_computation.3 | async-start | bytes 4194304 | tf_op jit(solution)/shard_map/all_to_all | solution.py:206
  306.9 35.1 %all-gather.10.cloned.1.call-done = bf16[1024,1024]{1,0:T(8,128)(2,1)} async-done(((bf16[1024,256]{1,0:T(8,128)(2,1)}), bf16[1024,1024]{1,0:T(8,128)(2,1)}) %all-gather.10.cloned.1.call-update) | async-done | bytes 2097168 | tf_op jit(solution)/shard_map/all_gather | solution.py:177
  342.0 4.1 %convolution_convert_fusion.1 = bf16[1024,512]{1,0:T(8,128)(2,1)} fusion(bf16[1024,1024]{1,0:T(8,128)(2,1)} %all-gather.10.cloned.1.call-done, bf16[1024,512]{1,0:T(8,128)(2,1)} %param.25), kind=kOutput, calls=%fused_computation.20 | convolution fusion | flops 1074266112 | bytes 4194304 | tf_op jit(solution)/shard_map/dot_general | solution.py:176
  346.1 8.6 %all-to-all-done.3 = bf16[64,8,2048]{2,1,0:T(8,128)(2,1)S(1)} async-done(((bf16[64,8,2048]{2,1,0:T(8,128)(2,1)}), bf16[64,8,2048]{2,1,0:T(8,128)(2,1)S(1)}, u32[]{:S(2)}, u32[]{:S(2)}) %all-to-all-start.3) | async-done | bytes 2097184 | tf_op jit(solution)/shard_map/all_to_all | solution.py:206
  356.0 3.5 gather_fusion.2
  (147 shorter events, 44.1 us)
Async XLA Ops:
  7.2 172.1 %copy-start = (bf16[1,512,2048]{2,1,0:T(8,128)(2,1)S(1)}, bf16[1,512,2048]{2,1,0:T(8,128)(2,1)}, u32[]{:S(2)}) copy-start(bf16[1,512,2048]{2,1,0:T(8,128)(2,1)} %param.33) | copy-start | bytes 6291460
  7.2 158.7 %all-gather.12.cloned.1.call-start = ((), (), s32[]{:S(2)}) async-start(), calls=%async_computation.7 | async-start | bytes 10485760 | tf_op jit(solution)/shard_map/all_gather | solution.py:194
  83.9 1.0 copy-start.9
  83.9 1.0 copy-start.14
  85.0 3.0 copy-start.12
  89.0 1.0 copy-start.5
  90.6 95.4 %all-to-all-start = ((f32[64,1,2,128]{3,2,1,0:T(2,128)}), f32[64,1,2,128]{3,2,1,0:T(2,128)S(1)}, u32[]{:S(2)}, u32[]{:S(2)}) async-start(f32[64,1,2,128]{3,2,1,0:T(2,128)} %broadcast_in_dim.86), calls=%async_computation | async-start | bytes 131072 | tf_op jit(solution)/shard_map/all_to_all | solution.py:19
  96.0 113.5 %all-gather.6.cloned.1.call-start = ((), (), s32[]{:S(2)}) async-start(), calls=%async_computation.4 | async-start | bytes 2359296 | tf_op jit(solution)/shard_map/all_gather | solution.py:38
  103.2 4.3 %copy-start.3 = (bf16[16,64,2,128]{3,2,1,0:T(2,128)(2,1)S(1)}, bf16[16,64,2,128]{3,2,1,0:T(2,128)(2,1)}, u32[]{:S(2)}) copy-start(bf16[16,64,2,128]{3,2,1,0:T(2,128)(2,1)} %reshape.258) | copy-start | bytes 1572868
  165.9 7.7 %copy-start.15 = (bf16[2048,2048]{1,0:T(8,128)(2,1)S(1)}, bf16[2048,2048]{1,0:T(8,128)(2,1)}, u32[]{:S(2)}) copy-start(bf16[2048,2048]{1,0:T(8,128)(2,1)} %all-gather.12.cloned.1.call-done) | copy-start | bytes 25165828
  165.9 7.7 %copy-start.16 = (bf16[1,2048,512]{2,1,0:T(8,128)(2,1)S(1)}, bf16[1,2048,512]{2,1,0:T(8,128)(2,1)}, u32[]{:S(2)}) copy-start(bf16[1,2048,512]{2,1,0:T(8,128)(2,1)} %param.32) | copy-start | bytes 6291460
  186.0 99.6 %all-to-all-start.2 = ((bf16[4,512,2048]{2,1,0:T(8,128)(2,1)}), bf16[4,512,2048]{2,1,0:T(8,128)(2,1)}, u32[]{:S(2)}, u32[]{:S(2)}) async-start(bf16[4,512,2048]{2,1,0:T(8,128)(2,1)} %bitcast.107), calls=%async_computation.2 | async-start | bytes 16777216 | tf_op jit(solution)/shard_map/all_to_all | solution.py:56
  191.6 37.3 %all-gather.8.cloned.1.call-start = ((), (), s32[]{:S(2)}) async-start(), calls=%async_computation.5 | async-start | bytes 6291456 | tf_op jit(solution)/shard_map/all_gather | solution.py:38
  231.5 2.9 copy-start.7
  231.5 2.9 copy-start.8
  234.3 1.1 copy-start.4
  234.3 1.2 copy-start.6
  292.8 61.8 %all-to-all-start.3 = ((bf16[64,8,2048]{2,1,0:T(8,128)(2,1)}), bf16[64,8,2048]{2,1,0:T(8,128)(2,1)S(1)}, u32[]{:S(2)}, u32[]{:S(2)}) async-start(bf16[64,8,2048]{2,1,0:T(8,128)(2,1)} %bitcast.109), calls=%async_computation.3 | async-start | bytes 4194304 | tf_op jit(solution)/shard_map/all_to_all | solution.py:206
  303.4 38.6 %all-gather.10.cloned.1.call-start = ((), (), s32[]{:S(2)}) async-start(), calls=%async_computation.6 | async-start | bytes 2621440 | tf_op jit(solution)/shard_map/all_gather | solution.py:177
  303.7 1.2 copy-start.10
  303.7 1.2 copy-start.13
  354.6 1.4 copy-start.2
  356.0 3.9 %copy-start.11 = (f32[2048]{0:T(1024)S(1)}, f32[2048]{0:T(1024)}, u32[]{:S(2)}) copy-start(f32[2048]{0:T(1024)} %param.30) | copy-start | bytes 24580
  356.0 5.0 %copy-start.1 = (bf16[1,512,2048]{2,1,0:T(8,128)(2,1)S(1)}, bf16[1,512,2048]{2,1,0:T(8,128)(2,1)}, u32[]{:S(2)}) copy-start(bf16[1,512,2048]{2,1,0:T(8,128)(2,1)} %param.33) | copy-start | bytes 6291460
Sparse Core Ops, SparseCore 0:
  84.1 81.7 all-gather.11
  167.7 41.8 all-gather.5
  211.4 17.5 all-gather.7
  306.3 35.6 all-gather.9
where the time goes:
time: 369 us; the launch traced here: 368 us
  waiting for transfers between devices  145 us (39%)
  blocking collectives  76.4 us (21%)
  other arithmetic  51.6 us (14%)
  matrix products  31.7 us (9%)
  local copies, waits for them, and re-layouts  26.6 us (7%)
  starting transfers between devices  22 us (6%)
  between operations  14.3 us (4%)
    all_to_all x1, blocking collectives, shards(): lax.all_to_all(packed, EP, split_axis=0, concat_axis=0, tiled=True)  63.2 us
    all_to_all x1, waiting for transfers between devices, sum_at_owner(): lax.all_to_all(in_blocks(shard, dim, length), axis, 0, 0, tiled=True)  48.2 us
    all_gather x2, waiting for transfers between devices, all_blocks(): tiles = lax.all_gather(tiles, axes[k], axis=0, tiled=True)  36.8 us
    all_gather x1, waiting for transfers between devices, shards(): lax.all_gather(state_layer_result, 'tp', axis=1, tiled=True)  35.1 us
    add x16, other arithmetic, advance(): return (jnp.exp(decay_log)[..., None] * state + addition, state)  16.4 us
    all_gather x1, waiting for transfers between devices, shards(): lax.all_gather(arrived.reshape(-1, arrived.shape[2]), 'tp', axis=0, tiled...  15.9 us
    all_gather x1, blocking collectives, all_blocks(): tiles = lax.all_gather(tiles, axes[k], axis=0, tiled=True)  13.2 us
    dynamic_update_slice x16, other arithmetic, shards(): lax.scan(advance, jnp.zeros((groups_each_device, HEAD, HEAD), jnp.float32...  10.6 us
  transfers between devices with their start and end apart: 7, of which 6 were waited for; matrix products, arithmetic and copies ran while one was open for 22% of the time, Pallas kernels for 0%

commit v1 on v0

--- a/solution.py
+++ b/solution.py
@@ -35,7 +35,8 @@
 def all_blocks(shard, axes, order):
     tiles = shard[None]
     for k in order:
-        tiles = lax.all_gather(tiles, axes[k], axis=0, tiled=True)
+        sent = jnp.stack([tiles] * lax.axis_size(axes[k]))
+        tiles = jnp.concatenate(lax.all_to_all(sent, axes[k], 0, 0), axis=0)
     current = [lax.axis_size(axes[k]) for k in reversed(order)]
     tiles = tiles.reshape(*current, *shard.shape)
     turned = sorted(range(len(order)), key=lambda place: order[len(order) - 1 - place])

time: 369 us -> 403 us (1.092)
  waiting for transfers between devices: 145 us -> 164 us
  starting transfers between devices: 22 us -> 34.3 us
  other arithmetic: 51.6 us -> 55.9 us
    all_to_all x1, waiting for transfers between devices: 48.2 us -> 85.3 us  [sum_at_owner(): lax.all_to_all(in_blocks(shard, dim, length), axis, 0, 0, tiled=True)]
    all_gather x2 -> x0, waiting for transfers between devices: 36.8 us -> none  [all_blocks(): tiles = lax.all_gather(tiles, axes[k], axis=0, tiled=True)]
    all_to_all x0 -> x1, waiting for transfers between devices: none -> 35.1 us  [shards(): lax.all_to_all(packed, EP, split_axis=0, concat_axis=0, tiled=True)]
    all_gather x1, waiting for transfers between devices: 15.9 us -> 0.01 us  [shards(): lax.all_gather(arrived.reshape(-1, arrived.shape[2]), 'tp', axis=0, tiled...]
    all_gather x1 -> x0, blocking collectives: 13.2 us -> none  [all_blocks(): tiles = lax.all_gather(tiles, axes[k], axis=0, tiled=True)]
    all_to_all x0 -> x1, starting transfers between devices: none -> 12.4 us  [shards(): lax.all_to_all(packed, EP, split_axis=0, concat_axis=0, tiled=True)]
    all_to_all x1 -> x3, blocking collectives: 63.2 us -> 75 us  [all_blocks(): tiles = jnp.concatenate(lax.all_to_all(sent, axes[k], 0, 0), axis=0)]
    another operation x3 -> x4, other arithmetic: 0.7 us -> 5.28 us  [the longest x1 4.58 us: all_blocks(): sent = jnp.stack([tiles] * lax.axis_size(axes[k]))]
  transfers between devices with their start and end apart: 7 -> 6, of which waited for: 6 -> 4; matrix products, arithmetic and copies ran while one was open for 22% -> 21% of each run, Pallas kernels for 0% -> 0%
where the time goes in v1:
time: 403 us; the launch traced here: 402 us
  waiting for transfers between devices  164 us (41%)
  blocking collectives  75 us (19%)
  other arithmetic  55.9 us (14%)
  starting transfers between devices  34.3 us (9%)
  matrix products  31.9 us (8%)
  local copies, waits for them, and re-layouts  25.5 us (6%)
  between operations  14.6 us (4%)
    all_to_all x1, waiting for transfers between devices, sum_at_owner(): lax.all_to_all(in_blocks(shard, dim, length), axis, 0, 0, tiled=True)  85.3 us
    all_to_all x3, blocking collectives, all_blocks(): tiles = jnp.concatenate(lax.all_to_all(sent, axes[k], 0, 0), axis=0)  75 us
    all_gather x1, waiting for transfers between devices, shards(): lax.all_gather(state_layer_result, 'tp', axis=1, tiled=True)  35.3 us
    all_to_all x1, waiting for transfers between devices, shards(): lax.all_to_all(packed, EP, split_axis=0, concat_axis=0, tiled=True)  35.1 us
    add x16, other arithmetic, advance(): return (jnp.exp(decay_log)[..., None] * state + addition, state)  16.5 us
    all_to_all x1, starting transfers between devices, shards(): lax.all_to_all(packed, EP, split_axis=0, concat_axis=0, tiled=True)  12.4 us
    dynamic_update_slice x16, other arithmetic, shards(): lax.scan(advance, jnp.zeros((groups_each_device, HEAD, HEAD), jnp.float32...  10.6 us
    all_to_all x1, starting transfers between devices, shards(): lax.all_to_all(finished, EP, split_axis=0, concat_axis=0, tiled=True)  10.4 us
  transfers between devices with their start and end apart: 6, of which 4 were waited for; matrix products, arithmetic and copies ran while one was open for 21% of the time, Pallas kernels for 0%

profile of v1, /device:TPU:8, one launch (start us, length us, event | category | flops | bytes accessed | tf_op | source)
XLA Modules:
  0.0 401.5 jit_solution(9616802578044558012)
XLA Ops:
  9.9 1.4 scatter_custom_fusion.1
  12.6 1.5 scatter_custom_fusion
  15.5 3.3 gather_fusion
  18.8 3.1 bitcast_select_fusion
  21.9 12.4 %all-to-all-start.4 = ((bf16[64,8,2048]{2,1,0:T(8,128)(2,1)}), bf16[64,8,2048]{2,1,0:T(8,128)(2,1)}, u32[]{:S(2)}, u32[]{:S(2)}) async-start(bf16[64,8,2048]{2,1,0:T(8,128)(2,1)} %bitcast_select_fusion), calls=%async_computation.4 | async-start | bytes 4194304 | tf_op jit(solution)/shard_map/all_to_all | solution.py:194
  35.7 1.7 reshape.259
  37.6 2.3 fusion.12
  39.9 2.7 reshape.258
  42.7 2.0 reshape.261
  45.9 2.7 bitcast_multiply_fusion.5
  48.5 1.9 fusion.25
  50.4 35.1 %all-to-all-done.4 = bf16[64,8,2048]{2,1,0:T(8,128)(2,1)} async-done(((bf16[64,8,2048]{2,1,0:T(8,128)(2,1)}), bf16[64,8,2048]{2,1,0:T(8,128)(2,1)}, u32[]{:S(2)}, u32[]{:S(2)}) %all-to-all-start.4) | async-done | bytes 2097184 | tf_op jit(solution)/shard_map/all_to_all | solution.py:194
  85.5 27.6 %while.13 = (s32[]{:T(128)}, f32[2,128,128]{2,1,0:T(8,128)S(1)}, f32[16,2,128,128]{3,2,1,0:T(8,128)}, f32[16,2,128]{2,1,0:T(2,128)S(1)}, f32[16,2,128,128]{3,2,1,0:T(8,128)}, /*index=5*/s32[]{:T(128)}, s32[]{:T(128)}) while((s32[]{:T(128)}, f32[2,128,128]{2,1,0:T(8,128)S(1)}, f32[16,2,128,128]{3,2,1,0:T(8,128)}, ...), condition=%wide.region_2.3_spmd.clone, body=%wide.region_1.2_spmd.clone.sunk | while | flops 131075 | bytes 659040 | solution.py:148
  113.2 9.8 %all_to_all.35 = bf16[4,1,1,2,128,128]{5,4,3,2,1,0:T(8,128)(2,1)S(1)} all-to-all(bf16[4,1,1,2,128,128]{5,4,3,2,1,0:T(8,128)(2,1)S(1)} %stack.9), channel_id=1, replica_groups=mesh['ep_0'=8,'ep_1'=4,'ep_2'=2,'tp'=4] {'ep_1'}, dimensions={0} | all-to-all | bytes 524288 | tf_op jit(solution)/shard_map/all_to_all | solution.py:39
  123.5 53.4 %all_to_all.36 = bf16[8,4,1,2,128,128]{5,4,3,1,2,0:T(8,128)(2,1)} all-to-all(bf16[8,4,1,2,128,128]{5,4,3,1,2,0:T(8,128)(2,1)S(1)} %stack.10), channel_id=1, replica_groups=mesh['ep_0'=8,'ep_1'=4,'ep_2'=2,'tp'=4] {'ep_0'}, dimensions={0} | all-to-all | bytes 4194304 | tf_op jit(solution)/shard_map/all_to_all | solution.py:39
  177.5 5.3 %all-to-all-start = ((f32[64,1,2,128]{3,2,1,0:T(2,128)}), f32[64,1,2,128]{3,2,1,0:T(2,128)S(1)}, u32[]{:S(2)}, u32[]{:S(2)}) async-start(f32[64,1,2,128]{3,2,1,0:T(2,128)} %broadcast_in_dim.52), calls=%async_computation | async-start | bytes 131072 | tf_op jit(solution)/shard_map/all_to_all | solution.py:19
  182.8 4.6 %pad_maximum_fusion = bf16[2,32,1,2,128,128]{5,4,3,1,2,0:T(8,128)(2,1)} fusion(bf16[1,32,1,2,128,128]{5,4,3,1,2,0:T(8,128)(2,1)} %bitcast.107), kind=kLoop, calls=%fused_computation.9 | loop fusion | flops 2097152 | bytes 6291456 | tf_op jit(solution)/shard_map/stack | solution.py:38
  187.4 7.7 %fusion.4 = f32[2048,512]{1,0:T(8,128)S(1)} fusion(bf16[2048,2048]{1,0:T(8,128)(2,1)} %all-gather.5.cloned.1.call-done, bf16[1,2048,512]{2,1,0:T(8,128)(2,1)} %param.31), kind=kOutput, calls=%fused_computation.15 | convolution fusion | flops 4294967296 | bytes 14680064 | tf_op jit(solution)/shard_map/dot_general | solution.py:196
  195.1 5.6 %multiply_convert_fusion = bf16[2048,512]{1,0:T(8,128)(2,1)S(1)} fusion(f32[2048,512]{1,0:T(8,128)S(1)} %fusion.4, bf16[2048,2048]{1,0:T(8,128)(2,1)S(1)} %copy-done.15, bf16[1,2048,512]{2,1,0:T(8,128)(2,1)S(1)} %copy-done.16), kind=kOutput, calls=%fused_computation.12 | convolution fusion | flops 4305453056 | bytes 16777216 | tf_op jit(solution)/shard_map/dot_general | solution.py:197
  200.7 6.8 %convolution_convert_fusion = bf16[2048,2048]{1,0:T(8,128)(2,1)} fusion(bf16[2048,512]{1,0:T(8,128)(2,1)S(1)} %multiply_convert_fusion, bf16[1,512,2048]{2,1,0:T(8,128)(2,1)S(1)} %copy-done), kind=kOutput, calls=%fused_computation.8 | convolution fusion | flops 4299161600 | bytes 12582912 | tf_op jit(solution)/shard_map/dot_general | solution.py:200
  207.5 11.8 %all_to_all.37 = bf16[2,32,1,2,128,128]{5,4,3,1,2,0:T(8,128)(2,1)} all-to-all(bf16[2,32,1,2,128,128]{5,4,3,1,2,0:T(8,128)(2,1)} %pad_maximum_fusion), channel_id=1, replica_groups=mesh['ep_0'=8,'ep_1'=4,'ep_2'=2,'tp'=4] {'ep_2'}, dimensions={0} | all-to-all | bytes 8388608 | tf_op jit(solution)/shard_map/all_to_all | solution.py:39
  219.4 5.9 %all-to-all-start.5 = ((bf16[4,512,2048]{2,1,0:T(8,128)(2,1)}), bf16[4,512,2048]{2,1,0:T(8,128)(2,1)}, u32[]{:S(2)}, u32[]{:S(2)}) async-start(bf16[4,512,2048]{2,1,0:T(8,128)(2,1)} %bitcast.108), calls=%async_computation.5 | async-start | bytes 16777216 | tf_op jit(solution)/shard_map/all_to_all | solution.py:57
  225.7 2.5 copy.61
  228.3 2.8 fusion
  232.3 1.9 multiply_reduce_fusion.1
  234.2 85.3 %all-to-all-done.5 = bf16[4,512,2048]{2,1,0:T(8,128)(2,1)} async-done(((bf16[4,512,2048]{2,1,0:T(8,128)(2,1)}), bf16[4,512,2048]{2,1,0:T(8,128)(2,1)}, u32[]{:S(2)}, u32[]{:S(2)}) %all-to-all-start.5) | async-done | bytes 8388640 | tf_op jit(solution)/shard_map/all_to_all | solution.py:57
  319.4 7.2 %reduce_sum.70 = bf16[512,2048]{1,0:T(8,128)(2,1)} reduce(bf16[4,512,2048]{2,1,0:T(8,128)(2,1)} %all-to-all-done.5, bf16[]{:T(256)} %constant.117.clone.1), dimensions={0}, to_apply=%region_13.14 | reduce | flops 3145728 | bytes 10485762 | tf_op jit(solution)/shard_map/reduce_sum | solution.py:58
  326.7 10.4 %all-to-all-start.6 = ((bf16[64,8,2048]{2,1,0:T(8,128)(2,1)}), bf16[64,8,2048]{2,1,0:T(8,128)(2,1)S(1)}, u32[]{:S(2)}, u32[]{:S(2)}) async-start(bf16[64,8,2048]{2,1,0:T(8,128)(2,1)} %bitcast.109), calls=%async_computation.6 | async-start | bytes 4194304 | tf_op jit(solution)/shard_map/all_to_all | solution.py:207
  340.7 35.3 %all-gather.3.cloned.1.call-done = bf16[1024,1024]{1,0:T(8,128)(2,1)} async-done(((bf16[1024,256]{1,0:T(8,128)(2,1)}), bf16[1024,1024]{1,0:T(8,128)(2,1)}) %all-gather.3.cloned.1.call-update) | async-done | bytes 2097168 | tf_op jit(solution)/shard_map/all_gather | solution.py:178
  376.0 4.1 %convolution_convert_fusion.1 = bf16[1024,512]{1,0:T(8,128)(2,1)} fusion(bf16[1024,1024]{1,0:T(8,128)(2,1)} %all-gather.3.cloned.1.call-done, bf16[1024,512]{1,0:T(8,128)(2,1)} %param.25), kind=kOutput, calls=%fused_computation.21 | convolution fusion | flops 1074266112 | bytes 4194304 | tf_op jit(solution)/shard_map/dot_general | solution.py:177
  380.1 8.2 %all-to-all-done.6 = bf16[64,8,2048]{2,1,0:T(8,128)(2,1)S(1)} async-done(((bf16[64,8,2048]{2,1,0:T(8,128)(2,1)}), bf16[64,8,2048]{2,1,0:T(8,128)(2,1)S(1)}, u32[]{:S(2)}, u32[]{:S(2)}) %all-to-all-start.6) | async-done | bytes 2097184 | tf_op jit(solution)/shard_map/all_to_all | solution.py:207
  389.7 3.5 gather_fusion.2
  (147 shorter events, 44.4 us)
Async XLA Ops:
  7.2 193.6 %copy-start = (bf16[1,512,2048]{2,1,0:T(8,128)(2,1)S(1)}, bf16[1,512,2048]{2,1,0:T(8,128)(2,1)}, u32[]{:S(2)}) copy-start(bf16[1,512,2048]{2,1,0:T(8,128)(2,1)} %param.33) | copy-start | bytes 6291460
  21.9 12.5 %copy-start.9 = (bf16[1024,256]{1,0:T(8,128)(2,1)S(1)}, bf16[1024,256]{1,0:T(8,128)(2,1)}, u32[]{:S(2)}) copy-start(bf16[1024,256]{1,0:T(8,128)(2,1)} %param.19) | copy-start | bytes 1572868
  21.9 12.5 %copy-start.14 = (f32[256]{0:T(256)S(1)}, f32[256]{0:T(256)}, u32[]{:S(2)}) copy-start(f32[256]{0:T(256)} %param.22) | copy-start | bytes 3076
  21.9 63.6 %all-to-all-start.4 = ((bf16[64,8,2048]{2,1,0:T(8,128)(2,1)}), bf16[64,8,2048]{2,1,0:T(8,128)(2,1)}, u32[]{:S(2)}, u32[]{:S(2)}) async-start(bf16[64,8,2048]{2,1,0:T(8,128)(2,1)} %bitcast_select_fusion), calls=%async_computation.4 | async-start | bytes 4194304 | tf_op jit(solution)/shard_map/all_to_all | solution.py:194
  34.4 3.1 copy-start.12
  34.4 153.0 %all-gather.5.cloned.1.call-start = ((), (), s32[]{:S(2)}) async-start(), calls=%async_computation.8 | async-start | bytes 10485760 | tf_op jit(solution)/shard_map/all_gather | solution.py:195
  44.6 1.2 copy-start.5
  45.9 2.7 copy-start.3
  177.5 30.0 %all-to-all-start = ((f32[64,1,2,128]{3,2,1,0:T(2,128)}), f32[64,1,2,128]{3,2,1,0:T(2,128)S(1)}, u32[]{:S(2)}, u32[]{:S(2)}) async-start(f32[64,1,2,128]{3,2,1,0:T(2,128)} %broadcast_in_dim.52), calls=%async_computation | async-start | bytes 131072 | tf_op jit(solution)/shard_map/all_to_all | solution.py:19
  187.4 7.7 %copy-start.15 = (bf16[2048,2048]{1,0:T(8,128)(2,1)S(1)}, bf16[2048,2048]{1,0:T(8,128)(2,1)}, u32[]{:S(2)}) copy-start(bf16[2048,2048]{1,0:T(8,128)(2,1)} %all-gather.5.cloned.1.call-done) | copy-start | bytes 25165828
  187.4 7.7 %copy-start.16 = (bf16[1,2048,512]{2,1,0:T(8,128)(2,1)S(1)}, bf16[1,2048,512]{2,1,0:T(8,128)(2,1)}, u32[]{:S(2)}) copy-start(bf16[1,2048,512]{2,1,0:T(8,128)(2,1)} %param.32) | copy-start | bytes 6291460
  219.4 100.1 %all-to-all-start.5 = ((bf16[4,512,2048]{2,1,0:T(8,128)(2,1)}), bf16[4,512,2048]{2,1,0:T(8,128)(2,1)}, u32[]{:S(2)}, u32[]{:S(2)}) async-start(bf16[4,512,2048]{2,1,0:T(8,128)(2,1)} %bitcast.108), calls=%async_computation.5 | async-start | bytes 16777216 | tf_op jit(solution)/shard_map/all_to_all | solution.py:57
  228.2 2.9 copy-start.7
  228.2 2.9 copy-start.8
  231.1 1.1 copy-start.4
  231.1 1.2 copy-start.6
  326.7 61.7 %all-to-all-start.6 = ((bf16[64,8,2048]{2,1,0:T(8,128)(2,1)}), bf16[64,8,2048]{2,1,0:T(8,128)(2,1)S(1)}, u32[]{:S(2)}, u32[]{:S(2)}) async-start(bf16[64,8,2048]{2,1,0:T(8,128)(2,1)} %bitcast.109), calls=%async_computation.6 | async-start | bytes 4194304 | tf_op jit(solution)/shard_map/all_to_all | solution.py:207
  337.1 38.9 %all-gather.3.cloned.1.call-start = ((), (), s32[]{:S(2)}) async-start(), calls=%async_computation.7 | async-start | bytes 2621440 | tf_op jit(solution)/shard_map/all_gather | solution.py:178
  337.4 1.2 copy-start.10
  337.4 1.2 copy-start.13
  388.3 1.4 copy-start.2
  389.7 3.9 copy-start.11
  389.7 5.0 %copy-start.1 = (bf16[1,512,2048]{2,1,0:T(8,128)(2,1)S(1)}, bf16[1,512,2048]{2,1,0:T(8,128)(2,1)}, u32[]{:S(2)}) copy-start(bf16[1,512,2048]{2,1,0:T(8,128)(2,1)} %param.33) | copy-start | bytes 6291460
Sparse Core Ops, SparseCore 0:
  85.7 81.7 all-gather.4
  340.3 35.6 all-gather.2
